TPU v7x, 128 devices: a whole 4x4x4 slice. The times are simulated.
128 devices in a mesh: sp: 16 (over z, y), tp: 8 (over x, core).
Axes of the slice: x: 4, y: 4, z: 4, core: 2. Of those that a mesh axis runs over, the one named last changes fastest.
Arguments:
- queries: bfloat16 [16384, 1024], P('sp', 'tp'), may hold values from -6 to 6
- keys: bfloat16 [16384, 1024], P('sp', 'tp'), may hold values from -6 to 6
- values: bfloat16 [16384, 1024], P('sp', 'tp'), may hold values from -6 to 6
- cum_gates: float32 [16384, 16], P('sp', 'tp'), may hold values from -2050 to 0, as said below
- doc_ids: int32 [16384], P('sp'), may hold values from 0 to 1, never falling along the last dimension, each value on 1 to 12288 neighbouring positions
- residual: bfloat16 [16384, 2048], P('sp', 'tp'), may hold values from -100 to 100
- w_out: bfloat16 [1024, 2048], P('tp'), may hold values from -0.1875 to 0.1875
- norm_gain: bfloat16 [2048], P('tp'), may hold values from 0.099609375 to 1.8984375
- w_up: bfloat16 [2048, 8192], P('sp', 'tp'), may hold values from -0.125 to 0.125
- w_down: bfloat16 [8192, 2048], P('tp', 'sp'), may hold values from -0.0625 to 0.0625
Outputs:
- output: bfloat16 [16384, 2048], P('sp', 'tp')
Inputs may be any that keep to these rules, and one draw needn't show every extreme that they name: `cum_gates`: along positions each head's values never rise. `doc_ids`: document numbers never fall along positions; a document holds 1 to three quarters of 16384 positions.
All inputs are finite; a program needn't handle non-finite values.
Results may differ from a plain program's by a relative error of at most 0.015.
Values may be sent and summed in bfloat16 or wider, within the bound.
A program may use at most 128 MiB of HBM per device.

v0:
```python
import math

import jax
import jax.numpy as jnp
from jax import lax
from jax.sharding import PartitionSpec as P

D = 2048
HD = 64


eps = 1e-06
far_below = -1e30


def gather_turned(arrays, axis, dims):
    turned = [jnp.moveaxis(a, dim, 0) for a, dim in zip(arrays, dims)]
    widths = [t[0].size for t in turned]
    both = jnp.concatenate([t.reshape(-1, w) for t, w in zip(turned, widths)], axis=1)
    whole = lax.all_gather(both, axis, axis=0, tiled=True)
    parts = jnp.split(whole, [sum(widths[:k]) for k in range(1, len(widths))], axis=1)
    return tuple(
        (
            jnp.moveaxis(b.reshape(-1, *t.shape[1:]), 0, dim)
            for b, t, dim in zip(parts, turned, dims)
        )
    )


def joined_along(parts, dim):
    dims = list(parts.shape[1:])
    dims[dim] *= parts.shape[0]
    return jnp.moveaxis(parts, 0, dim).reshape(dims)


def copy_for_each(value, axis):
    peers = lax.axis_size(axis)
    return lax.all_to_all(
        jnp.broadcast_to(value[None], (peers, *value.shape)), axis, 0, 0, tiled=True
    )


def gather_directly(value, axis, dim):
    return joined_along(copy_for_each(value, axis), dim)


def side_by_side(arrays, axis, dim, along):
    both = jnp.concatenate(arrays, axis=along)
    whole, at, outs = (lax.all_gather(both, axis, axis=dim, tiled=True), 0, [])
    for a in arrays:
        outs.append(lax.slice_in_dim(whole, at, at + a.shape[along], axis=along))
        at += a.shape[along]
    return tuple(outs)


def taken_together(value, axis):
    everything = copy_for_each(value, axis)
    return jnp.sum(everything, axis=0)


def attend_span(state_carry, context, key_blk, value_blk, document_block, gate_blk, key_start):
    queries_three, gate_rows, doc_rows, q_pos = context
    running_max, weight_sum, accumulated = state_carry
    key_span = key_blk.shape[0]
    head_count = queries_three.shape[1]
    key_three = key_blk.reshape(key_span, head_count, HD)
    value_three = value_blk.reshape(key_span, head_count, HD)
    key_pos = key_start + jnp.arange(key_span, dtype=jnp.int32)
    scores = jnp.einsum(
        "qhd,khd->hqk", queries_three, key_three, preferred_element_type=jnp.float32
    ) * HD ** (-0.5)
    scores = scores + gate_rows[:, :, None] - gate_blk[:, None, :]
    visible = (
        (key_pos[None, :] <= q_pos[:, None]) & (document_block[None, :] == doc_rows[:, None])
    )[None]
    masked = jnp.where(visible, scores, far_below)
    new_max = jnp.maximum(running_max, jnp.max(masked, axis=-1))
    weights = jnp.where(visible, jnp.exp(masked - new_max[..., None]), 0.0)
    shrink = jnp.exp(running_max - new_max)
    weight_sum = weight_sum * shrink + jnp.sum(weights, axis=-1)
    product = jnp.einsum(
        "hqk,khd->hqd",
        weights.astype(jnp.bfloat16),
        value_three,
        preferred_element_type=jnp.float32,
    )
    accumulated = accumulated * shrink[..., None] + product
    return (new_max, weight_sum, accumulated)


def fold_piece(state_carry, context, shard_piece, gates_t):
    key_piece, value_piece, doc_piece = shard_piece
    piece_rows = key_piece.shape[0]
    key_span = math.gcd(piece_rows, 1024)
    q_last = context[3][-1]
    doc_first = context[2][0]

    def key_step(step_index, inner_carry):
        offset = step_index * key_span
        key_blk = lax.dynamic_slice_in_dim(key_piece, offset, key_span, 0)
        value_blk = lax.dynamic_slice_in_dim(value_piece, offset, key_span, 0)
        document_block = lax.dynamic_slice_in_dim(doc_piece, offset, key_span, 0)
        gate_blk = lax.dynamic_slice_in_dim(gates_t, jnp.maximum(offset, 0), key_span, 1)
        live = (offset >= 0) & (offset <= q_last) & (document_block[-1] >= doc_first)

        def compute(given):
            return attend_span(given, context, key_blk, value_blk, document_block, gate_blk, offset)

        def passing(given):
            return given

        return lax.cond(live, compute, passing, inner_carry)

    return lax.fori_loop(0, piece_rows // key_span, key_step, state_carry)


def body(queries, keys, values, cum_gates, doc_ids, residual, w_out, norm_gain, w_up, w_down):
    tok_rows = queries.shape[0]
    head_cols = queries.shape[1]
    head_count = head_cols // HD
    row_start = lax.axis_index("sp") * tok_rows
    up_whole, down_whole = gather_turned((w_up, w_down), "sp", (0, 1))
    proj_cols = lax.all_to_all(w_out, "tp", split_axis=1, concat_axis=0, tiled=True)
    gates_t = jnp.transpose(gather_directly(cum_gates, "sp", 0))
    q_pos = row_start + jnp.arange(tok_rows, dtype=jnp.int32)
    context = (queries.reshape(tok_rows, head_count, HD), jnp.transpose(cum_gates), doc_ids, q_pos)
    start_carry = (
        jnp.full((head_count, tok_rows), far_below, jnp.float32),
        jnp.zeros((head_count, tok_rows), jnp.float32),
        jnp.zeros((head_count, tok_rows, HD), jnp.float32),
    )
    running_max, weight_sum, accumulated = fold_piece(
        start_carry,
        context,
        (
            *side_by_side((keys, values), "sp", 0, 1),
            lax.all_gather(doc_ids, "sp", axis=0, tiled=True),
        ),
        gates_t,
    )
    attended = (accumulated / weight_sum[..., None]).astype(jnp.bfloat16)
    attended = jnp.transpose(attended, (1, 0, 2)).reshape(tok_rows, head_cols)
    group_total = lax.axis_size("tp")
    attended_whole = gather_directly(attended, "tp", 1)
    attended_groups = jnp.transpose(
        attended_whole.reshape(tok_rows, group_total, head_cols), (1, 0, 2)
    )
    proj_groups = proj_cols.reshape(group_total, head_cols, proj_cols.shape[1])
    group_terms = jnp.einsum(
        "gtc,gcd->gtd", attended_groups, proj_groups, preferred_element_type=jnp.float32
    )
    head_mixed = jnp.sum(group_terms.astype(jnp.bfloat16).astype(jnp.float32), axis=0)
    middle = (residual.astype(jnp.float32) + head_mixed).astype(jnp.bfloat16)
    middle_wide = middle.astype(jnp.float32)
    row_squares = taken_together(jnp.sum(middle_wide * middle_wide, axis=-1), "tp")
    scaled = middle_wide * lax.rsqrt(row_squares[:, None] / D + eps)
    normed = (scaled * norm_gain.astype(jnp.float32)).astype(jnp.bfloat16)
    features = lax.all_gather(normed, "tp", axis=1, tiled=True)
    up_proj = jnp.dot(features, up_whole, preferred_element_type=jnp.float32)
    hidden = jnp.square(jax.nn.relu(up_proj)).astype(jnp.bfloat16)
    down_terms = jnp.dot(hidden, down_whole, preferred_element_type=jnp.float32)
    feed = lax.psum_scatter(
        down_terms.astype(jnp.bfloat16), "tp", scatter_dimension=1, tiled=True
    ).astype(jnp.float32)
    return (middle_wide + feed).astype(jnp.bfloat16)


def solution(mesh):
    in_specs = (
        P("sp", "tp"),
        P("sp", "tp"),
        P("sp", "tp"),
        P("sp", "tp"),
        P("sp"),
        P("sp", "tp"),
        P("tp", None),
        P("tp"),
        P("sp", "tp"),
        P("tp", "sp"),
    )
    out_specs = P("sp", "tp")
    return jax.shard_map(body, mesh=mesh, in_specs=in_specs, out_specs=out_specs, check_vma=False)
```

profile of v0, /device:TPU:0, one launch (start us, length us, event | category | flops | bytes accessed | tf_op | source)
XLA Modules:
  0.0 400.7 jit_solution(2995979391306129125)
XLA Ops:
  6.5 1.1 copy.43
  7.6 1.1 copy.42
  8.7 0.8 pad_maximum_fusion
  9.6 1.1 copy.49
  10.8 1.8 pad_maximum_fusion.1
  12.6 1.4 broadcast_in_dim.65
  14.0 8.2 %all-to-all-start = ((f32[16,1024,2]{1,2,0:T(2,128)}), f32[16,1024,2]{1,2,0:T(2,128)S(1)}, u32[]{:S(2)}, u32[]{:S(2)}) async-start(f32[16,1024,2]{1,2,0:T(2,128)} %broadcast_in_dim.65), calls=%async_computation | async-start | bytes 262144 | tf_op jit(solution)/shard_map/all_to_all | solution.py:38
  22.2 0.7 slice.19
  22.8 1.2 slice.20
  24.1 1.1 copy.44
  25.2 1.3 copy.46
  26.5 1.0 copy.47
  27.5 24.3 %all_gather.12 = s32[16384]{0:T(1024)S(1)} all-gather(s32[1024]{0:T(1024)} %param.18), channel_id=1, replica_groups=mesh['sp'=16,'tp'=8] {'sp'}, dimensions={0}, use_global_device_ids=true | all-gather | bytes 69632 | tf_op jit(solution)/shard_map/all_gather | solution.py:137
  51.8 4.3 %all-to-all-start.2 = ((bf16[128,8,256]{2,0,1:T(8,128)(2,1)}), bf16[128,8,256]{2,0,1:T(8,128)(2,1)S(1)}, u32[]{:S(2)}, u32[]{:S(2)}) async-start(bf16[128,8,256]{2,0,1:T(8,128)(2,1)} %copy.47), calls=%async_computation.2 | async-start | bytes 1048576 | tf_op jit(solution)/shard_map/all_to_all | solution.py:123
  56.2 27.8 %all-gather.4.cloned.1.call-done = bf16[16384,256]{0,1:T(8,128)(2,1)} async-done(((bf16[1024,256]{0,1:T(8,128)(2,1)}), bf16[16384,256]{0,1:T(8,128)(2,1)}) %all-gather.4.cloned.1.call-update) | async-done | bytes 8388624 | tf_op jit(solution)/shard_map/all_gather | solution.py:49
  84.0 5.8 %fusion.28 = (bf16[16384,128]{0,1:T(8,128)(2,1)}, bf16[16384,128]{0,1:T(8,128)(2,1)}) fusion(bf16[16384,256]{0,1:T(8,128)(2,1)} %all-gather.4.cloned.1.call-done), kind=kLoop, calls=%fused_computation.41 | loop fusion | bytes 16777216 | tf_op jit(solution)/shard_map/slice | solution.py:51
  89.9 51.8 %while.18 = (s32[]{:T(128)}, f32[2,1024]{1,0:T(2,128)S(1)}, f32[2,1024]{1,0:T(2,128)S(1)}, f32[2,1024,64]{1,2,0:T(8,128)S(1)}, s32[]{:T(128)}, /*index=5*/s32[16...) while((s32[]{:T(128)}, f32[2,1024]{1,0:T(2,128)S(1)}, ...), condition=%wide.region_5.6_spmd.clone, body=%wide.region_0.5_spmd.clone.sunk | while | flops 580130816 | bytes 32481744 | solution.py:114
  90.6 0.6 slice.29
  92.4 11.0 %conditional.3 = ((f32[2,1024]{1,0:T(2,128)S(1)}, f32[2,1024]{1,0:T(2,128)S(1)}, f32[2,1024,64]{1,2,0:T(8,128)S(1)})) conditional(s32[]{:T(128)} %convert_element_type.88, (f32[2,1024]{1,0:T(2,128)S(1)}, f32[2,1024]{1,0:T(2,128)S(1)}, f32[2,1024,64]{1,2,0:T(8,128)S(1)}) %tuple.50, (s32[]{:T(128)}, s32[]{:T(128)}, s32[1024]{0:T(1024)S(1)}, ...), branch_computations={%region_1.0_spmd, %region_2.4_spmd} | conditional | flops 580130816 | bytes 32469052 | solution.py:112
  92.5 1.2 compare_and_fusion
  93.7 1.1 constant_dynamic-slice_fusion
  94.8 2.4 fusion.4
  97.2 3.0 fusion.3
  100.2 3.2 fusion.8
  104.2 0.6 slice.29
  106.7 0.6 slice.29
  109.3 0.6 slice.29
  111.8 0.6 slice.29
  114.4 0.6 slice.29
  116.9 0.6 slice.29
  119.5 0.6 slice.29
  122.0 0.6 slice.29
  124.5 0.6 slice.29
  127.1 0.6 slice.29
  129.6 0.6 slice.29
  132.2 0.6 slice.29
  137.3 0.6 slice.29
  142.2 31.3 %all_to_all.32 = bf16[8,1024,128]{2,1,0:T(8,128)(2,1)S(1)} all-to-all(bf16[8,1024,128]{2,1,0:T(8,128)(2,1)S(1)} %broadcast_in_dim.67), channel_id=1, replica_groups=mesh['sp'=16,'tp'=8] {'tp'}, dimensions={0} | all-to-all | bytes 4194304 | tf_op jit(solution)/shard_map/all_to_all | solution.py:38
  173.4 1.2 convert_reduce_fusion
  174.9 0.6 broadcast_in_dim.68
  175.6 3.3 all-to-all-start.3
  179.2 5.1 %all-to-all-done.3 = f32[8,1,1024]{2,1,0:T(1,128)S(1)} async-done(((f32[8,1,1024]{2,1,0:T(1,128)}), f32[8,1,1024]{2,1,0:T(1,128)S(1)}, u32[]{:S(2)}, u32[]{:S(2)}) %all-to-all-start.3) | async-done | bytes 32800 | tf_op jit(solution)/shard_map/all_to_all | solution.py:38
  184.3 1.0 fusion.25
  185.4 153.6 %all-gather.6.cloned.1.call-done = bf16[1024,2048]{1,0:T(8,128)(2,1)} async-done(((bf16[1024,256]{1,0:T(8,128)(2,1)}), bf16[1024,2048]{1,0:T(8,128)(2,1)}) %all-gather.6.cloned.1.call-update) | async-done | bytes 4194320 | tf_op jit(solution)/shard_map/all_gather | solution.py:158
  339.0 8.1 %multiply_convert_fusion = bf16[1024,1024]{1,0:T(8,128)(2,1)S(1)} fusion(bf16[1024,2048]{1,0:T(8,128)(2,1)} %all-gather.6.cloned.1.call-done, bf16[2048,2048]{0,1:T(8,128)(2,1)} %all-gather.8.cloned.1.call-done), kind=kOutput, calls=%fused_computation.25 | convolution fusion | flops 4298113024 | bytes 10485760 | tf_op jit(solution)/shard_map/dot_general | solution.py:159
  347.2 6.1 %fusion.18 = bf16[1024,2048]{1,0:T(8,128)(2,1)} fusion(bf16[1024,1024]{1,0:T(8,128)(2,1)S(1)} %multiply_convert_fusion, bf16[2048,2048]{0,1:T(8,128)(2,1)S(1)} %copy-done.3), kind=kOutput, calls=%fused_computation.26 | convolution fusion | flops 4297064448 | bytes 10485760 | tf_op jit(solution)/shard_map/dot_general | solution.py:161
  353.3 39.0 %reduce-scatter.2.cloned.1.call-done = bf16[1024,256]{1,0:T(8,128)(2,1)} async-done(((bf16[1024,2048]{1,0:T(8,128)(2,1)}), bf16[1024,256]{1,0:T(8,128)(2,1)}) %reduce-scatter.2.cloned.1.call-update) | async-done | bytes 524304 | tf_op jit(solution)/shard_map/reduce_scatter | solution.py:162
  392.2 2.0 fusion.26
  (86 shorter events, 2.9 us)
Async XLA Ops:
  6.5 77.4 %all-gather.4.cloned.1.call-start = ((), (), s32[]{:S(2)}) async-start(), calls=%async_computation.5 | async-start | bytes 8912896 | tf_op jit(solution)/shard_map/all_gather | solution.py:49
  9.6 175.9 %all-gather.8.cloned.1.call-start = ((), (), s32[]{:S(2)}) async-start(), calls=%async_computation.7 | async-start | bytes 8912896 | tf_op jit(solution)/shard_map/all_gather | solution.py:20
  14.0 37.8 %all-to-all-start = ((f32[16,1024,2]{1,2,0:T(2,128)}), f32[16,1024,2]{1,2,0:T(2,128)S(1)}, u32[]{:S(2)}, u32[]{:S(2)}) async-start(f32[16,1024,2]{1,2,0:T(2,128)} %broadcast_in_dim.65), calls=%async_computation | async-start | bytes 262144 | tf_op jit(solution)/shard_map/all_to_all | solution.py:38
  51.8 90.1 %all-to-all-start.2 = ((bf16[128,8,256]{2,0,1:T(8,128)(2,1)}), bf16[128,8,256]{2,0,1:T(8,128)(2,1)S(1)}, u32[]{:S(2)}, u32[]{:S(2)}) async-start(bf16[128,8,256]{2,0,1:T(8,128)(2,1)} %copy.47), calls=%async_computation.2 | async-start | bytes 1048576 | tf_op jit(solution)/shard_map/all_to_all | solution.py:123
  56.2 33.7 %copy-start.1 = (f32[1024,2]{0,1:T(2,128)S(1)}, f32[1024,2]{0,1:T(2,128)}, u32[]{:S(2)}) copy-start(f32[1024,2]{0,1:T(2,128)} %param.17) | copy-start | bytes 24580
  56.2 33.7 %copy-start.2 = (s32[1024]{0:T(1024)S(1)}, s32[1024]{0:T(1024)}, u32[]{:S(2)}) copy-start(s32[1024]{0:T(1024)} %param.18) | copy-start | bytes 12292
  141.6 33.0 %copy-start = (bf16[1024,256]{1,0:T(8,128)(2,1)S(1)}, bf16[1024,256]{1,0:T(8,128)(2,1)}, u32[]{:S(2)}) copy-start(bf16[1024,256]{1,0:T(8,128)(2,1)} %param.19) | copy-start | bytes 1572868
  141.7 37.5 %copy-start.4 = (bf16[256]{0:T(256)(128)(2,1)S(1)}, bf16[256]{0:T(256)(128)(2,1)}, u32[]{:S(2)}) copy-start(bf16[256]{0:T(256)(128)(2,1)} %param.21) | copy-start | bytes 1540
  175.6 8.7 %all-to-all-start.3 = ((f32[8,1,1024]{2,1,0:T(1,128)}), f32[8,1,1024]{2,1,0:T(1,128)S(1)}, u32[]{:S(2)}, u32[]{:S(2)}) async-start(f32[8,1,1024]{2,1,0:T(1,128)} %broadcast_in_dim.68), calls=%async_computation.3 | async-start | bytes 65536 | tf_op jit(solution)/shard_map/all_to_all | solution.py:38
  178.9 160.1 %all-gather.6.cloned.1.call-start = ((), (), s32[]{:S(2)}) async-start(), calls=%async_computation.6 | async-start | bytes 4718592 | tf_op jit(solution)/shard_map/all_gather | solution.py:158
  185.4 206.9 %reduce-scatter.2.cloned.1.call-start = ((), (), s32[]{:S(2)}) async-start(), calls=%async_computation.8 | async-start | bytes 4718592 | tf_op jit(solution)/shard_map/reduce_scatter | solution.py:162
  339.0 8.1 %copy-start.3 = (bf16[2048,2048]{0,1:T(8,128)(2,1)S(1)}, bf16[2048,2048]{0,1:T(8,128)(2,1)}, u32[]{:S(2)}) copy-start(bf16[2048,2048]{0,1:T(8,128)(2,1)} %all-gather.8.cloned.1.call-done) | copy-start | bytes 25165828
Sparse Core Ops, SparseCore 0:
  9.7 74.2 all-gather.3
  86.1 76.9 all-gather.7
  185.5 153.4 all-gather.5
  353.4 38.8 reduce-scatter.1
where the time goes:
time: 397 us; the launch traced here: 401 us
  waiting for transfers between devices  226 us (57%)
  blocking collectives  55.6 us (14%)
  loops' own time  31.5 us (8%)
  local copies, waits for them, and re-layouts  27.4 us (7%)
  matrix products  21.1 us (5%)
  starting transfers between devices  16.1 us (4%)
  between operations  13.3 us (3%)
  other arithmetic  10.2 us (3%)
    all_gather x1, waiting for transfers between devices, body(): features = lax.all_gather(normed, 'tp', axis=1, tiled=True)  154 us
    reduce_scatter x1, waiting for transfers between devices, body(): lax.psum_scatter(down_terms.astype(jnp.bfloat16), 'tp', scatter_dimension...  39 us
    all_to_all x1, blocking collectives, copy_for_each(): lax.all_to_all(jnp.broadcast_to(value[None], (peers, *value.shape)), axis...  31.3 us
    another operation x1, loops' own time, fold_piece(): return lax.fori_loop(0, piece_rows // key_span, key_step, state_carry)  31.2 us
    all_gather x1, waiting for transfers between devices, side_by_side(): whole, at, outs = (lax.all_gather(both, axis, axis=dim, tiled=True), 0, [])  27.8 us
    all_gather x1, blocking collectives, body(): lax.all_gather(doc_ids, 'sp', axis=0, tiled=True)  24.3 us
    all_to_all x2, starting transfers between devices, copy_for_each(): lax.all_to_all(jnp.broadcast_to(value[None], (peers, *value.shape)), axis...  11.5 us
    slice x16, local copies, waits for them, and re-layouts, key_step(): document_block[-1] >= doc_first  9.14 us
  transfers between devices with their start and end apart: 7, of which 4 were waited for; matrix products, arithmetic and copies ran while one was open for 10% of the time, Pallas kernels for 0%

commit v1 on v0

v1 whole, which is shorter than its diff:
```python
import functools

import jax
import jax.numpy as jnp
from jax import lax
from jax.experimental import pallas as pl
from jax.experimental.pallas import tpu as pltpu
from jax.sharding import PartitionSpec as P

D = 2048
HD = 64
T = 1024
HALF = 512
ITEM = 576
eps = 1e-06
far_below = -1e30
BIG = 8192.0
MESH = pl.DeviceIdType.MESH
BF = jnp.bfloat16
F32 = jnp.float32
VM = pl.BlockSpec(memory_space=pltpu.VMEM)
HB = pl.BlockSpec(memory_space=pl.ANY)
DMA = pltpu.SemaphoreType.DMA


def sds(shape, dtype):
    return jax.ShapeDtypeStruct(shape, dtype)


def place():
    sp, tp = lax.axis_index("sp"), lax.axis_index("tp")
    return lax.div(sp, 4), lax.rem(sp, 4), lax.div(tp, 2), lax.rem(tp, 2)


def dev(z, y, x, c):
    return (z * 4 + y, x * 2 + c)


def send(src, dst, ssem, rsem, device):
    return pltpu.make_async_remote_copy(
        src_ref=src, dst_ref=dst, send_sem=ssem, recv_sem=rsem, device_id=device, device_id_type=MESH
    )


def up(v, k):
    return lax.rem(v + k, 4)


def pack_kernel(q_ref, k_ref, v_ref, g_ref, d_ref, qt_ref, kv_ref):
    qt = (q_ref[...].astype(F32) * (HD ** -0.5)).T.astype(BF)
    qt_ref[0] = qt[:HD]
    qt_ref[1] = qt[HD:]
    k_lo, k_hi = k_ref[:HALF].astype(F32), k_ref[HALF:].astype(F32)
    first = lax.broadcasted_iota(jnp.int32, (HALF, 128), 1) < HD
    kv_ref[0, 0, :HALF] = jnp.where(first, k_lo, pltpu.roll(k_hi, HD, 1)).astype(BF)
    kv_ref[0, 1, :HALF] = jnp.where(first, pltpu.roll(k_lo, HD, 1), k_hi).astype(BF)
    vt = v_ref[...].astype(F32).T.astype(BF)
    row = lax.broadcasted_iota(jnp.int32, (8, T), 0)
    doc0 = 1.0 - d_ref[...].astype(F32)
    for j in range(2):
        kv_ref[0, j, HALF:] = jnp.zeros((64, 128), BF)
        g = g_ref[j:j + 1, :]
        hi = g.astype(BF).astype(F32)
        mid = (g - hi).astype(BF).astype(F32)
        lo = (g - hi) - mid
        aux = jnp.where(row == 0, hi, jnp.where(row == 1, mid, jnp.where(row == 2, lo, jnp.where(row == 3, doc0, 0.0))))
        for n in range(8):
            kv_ref[1, j, n * 64:(n + 1) * 64] = vt[j * HD:(j + 1) * HD, n * 128:(n + 1) * 128]
        for n in range(4):
            two = jnp.concatenate([aux[:, (2 * n) * 128:(2 * n + 1) * 128], aux[:, (2 * n + 1) * 128:(2 * n + 2) * 128]], axis=0)
            kv_ref[1, j, HALF + n * 16:HALF + (n + 1) * 16] = two.astype(BF)


def pack(q, k, v, g, d):
    return pl.pallas_call(
        pack_kernel,
        out_shape=(sds((2, HD, T), BF), sds((2, 2, ITEM, 128), BF)),
        in_specs=[VM] * 5,
        out_specs=(VM, VM),
        name="pack",
    )(q, k, v, g, d)


def exchange_kernel(
    qt, kv, wo, res, gain, qin, kvall, woall, resin, gainall,
    qs, qr, ks, rr, s_sib, r_sib, s_r, s_l,
    wl, w_sib, wr_sib, w_s_r, w_s_l, w_r, es, er, gs, gr,
):
    z, y, x, c = place()
    sp, tp = z * 4 + y, x * 2 + c
    sib = dev(z, y, x, 1 - c)
    yp, ym, y2 = up(y, 1), up(y, 3), up(y, 2)
    xp, xm, x2 = up(x, 1), up(x, 3), up(x, 2)

    def guarded(is_self, local, remote):
        @pl.when(is_self)
        def _():
            local.start()

        @pl.when(jnp.logical_not(is_self))
        def _():
            remote.start()

    pending = []
    for j in range(2):
        zt = 2 * c + j
        for t in range(2):
            mine = (zt == z) & (c == t)
            src, dst = kv.at[t, j], kvall.at[t, sp]
            remote = send(src, dst, ks.at[2 * t + j], rr.at[sp], dev(zt, y, x, t))
            guarded(mine, pltpu.make_async_copy(src, dst, rr.at[sp]), remote)
            pending.append((mine, remote))
    for j in range(2):
        zt = 2 * c + j
        for hf in range(2):
            ct = lax.rem(hf + z, 2)
            mine = (zt == z) & (ct == c)
            src, dst = qt.at[j, :, pl.ds(hf * HALF, HALF)], qin.at[z]
            remote = send(src, dst, qs.at[2 * j + hf], qr.at[z], dev(zt, y, x, ct))
            guarded(mine, pltpu.make_async_copy(src, dst, qr.at[z]), remote)
            pending.append((mine, remote))

    done = []

    def wrows(xs, half):
        return pl.ds((2 * xs + c) * 128 + half * 64, 64)

    def go(copy):
        copy.start()
        done.append(copy)

    own_w = []
    for half in range(2):
        src, dst = wo.at[pl.ds(half * 64, 64)], woall.at[wrows(x, half)]
        n = 2 * x + half
        loc = pltpu.make_async_copy(src, dst, wl.at[half])
        loc.start()
        own_w.append(loc)
        go(send(src, dst, w_s_r.at[n], w_r.at[n], dev(z, y, xp, c)))
        go(send(src, dst, w_s_l.at[n], w_r.at[n], dev(z, y, xm, c)))
        go(send(src, dst, w_sib.at[n], wr_sib.at[n], sib))

    own_e = pltpu.make_async_copy(res.at[pl.ds(pl.multiple_of(tp * 128, 128), 128)],
                                  resin.at[:, pl.ds(pl.multiple_of(tp * 256, 256), 256)], er.at[tp])
    own_e.start()
    own_g = pltpu.make_async_copy(gain, gainall.at[:, pl.ds(pl.multiple_of(tp * 256, 256), 256)], gr.at[tp])
    own_g.start()
    for k in range(1, 8):
        to = lax.rem(tp + k, 8)
        cols = pl.ds(pl.multiple_of(tp * 256, 256), 256)
        go(send(res.at[pl.ds(pl.multiple_of(to * 128, 128), 128)], resin.at[:, cols], es.at[k], er.at[tp], (sp, to)))
        go(send(gain, gainall.at[:, cols], gs.at[k], gr.at[tp], (sp, to)))

    def arrived(b):
        send(kvall.at[c, b], kvall.at[c, b], s_sib.at[b], rr.at[b], sib).wait_recv()
        go(send(kvall.at[c, b], kvall.at[c, b], s_sib.at[b], r_sib.at[b], sib))

    def right(b):
        go(send(kvall.at[c, b], kvall.at[c, b], s_r.at[b], rr.at[b], dev(z, yp, x, c)))

    def left(b):
        go(send(kvall.at[c, b], kvall.at[c, b], s_l.at[b], rr.at[b], dev(z, ym, x, c)))

    zs = [z, up(z, 1), up(z, 3), up(z, 2)]

    def near(r):
        b = zs[r] * 4 + y
        arrived(b)
        right(b)
        left(b)

    def next_to(r):
        b = zs[r] * 4 + ym
        arrived(b)
        if r in (0, 2):
            right(b)
        b = zs[r] * 4 + yp
        arrived(b)
        if r in (1, 3):
            left(b)

    def w_arrived(xs, half):
        rows, n = wrows(xs, half), 2 * xs + half
        send(woall.at[rows], woall.at[rows], w_sib.at[n], w_r.at[n], sib).wait_recv()
        go(send(woall.at[rows], woall.at[rows], w_sib.at[n], wr_sib.at[n], sib))

    def w_next(half):
        w_arrived(xm, half)
        w_arrived(xp, half)
        if half == 0:
            rows, n = wrows(xm, 0), 2 * xm
            go(send(woall.at[rows], woall.at[rows], w_s_r.at[n], w_r.at[n], dev(z, y, xp, c)))
        else:
            rows, n = wrows(xp, 1), 2 * xp + 1
            go(send(woall.at[rows], woall.at[rows], w_s_l.at[n], w_r.at[n], dev(z, y, xm, c)))

    near(0)
    near(1)
    near(2)
    next_to(0)
    w_next(0)
    near(3)
    next_to(1)
    next_to(2)
    w_next(1)
    next_to(3)
    for r in range(4):
        arrived(zs[r] * 4 + y2)
    w_arrived(x2, 0)
    w_arrived(x2, 1)

    for b in range(16):
        send(kvall.at[1 - c, b], kvall.at[1 - c, b], s_sib.at[b], r_sib.at[b], sib).wait_recv()
    for n in range(8):
        rows = pl.ds((2 * (n // 2) + (1 - c)) * 128 + (n % 2) * 64, 64)
        send(woall.at[rows], woall.at[rows], w_sib.at[n], wr_sib.at[n], sib).wait_recv()
    for i in range(4):
        send(qin.at[i], qin.at[i], qs.at[0], qr.at[i], sib).wait_recv()
    for n in range(8):
        cols = pl.ds(n * 256, 256)
        send(resin.at[:, cols], resin.at[:, cols], es.at[0], er.at[n], sib).wait_recv()
        send(gainall.at[:, cols], gainall.at[:, cols], gs.at[0], gr.at[n], sib).wait_recv()
    for loc in own_w:
        loc.wait()
    for mine, remote in pending:
        @pl.when(jnp.logical_not(mine))
        def _():
            remote.wait_send()
    for copy in done:
        copy.wait_send()


def exchange(qt, kv, wo, res, gain):
    return pl.pallas_call(
        exchange_kernel,
        out_shape=(
            sds((4, HD, HALF), BF),
            sds((2, 16, ITEM, 128), BF),
            sds((1024, D), BF),
            sds((128, D), BF),
            sds((8, D), F32),
        ),
        in_specs=[VM] * 5,
        out_specs=(HB,) * 5,
        scratch_shapes=[
            DMA((4,)), DMA((4,)), DMA((4,)), DMA((16,)), DMA((16,)), DMA((16,)), DMA((16,)), DMA((16,)),
            DMA((2,)), DMA((8,)), DMA((8,)), DMA((8,)), DMA((8,)), DMA((8,)),
            DMA((8,)), DMA((8,)), DMA((8,)), DMA((8,)),
        ],
        compiler_params=pltpu.CompilerParams(has_side_effects=True),
        cost_estimate=pl.CostEstimate(flops=20_000_000_000, bytes_accessed=16_000_000, transcendentals=0),
        name="exchange",
    )(qt, kv, wo, res, gain)


def attend_kernel(q_ref, kv_ref, o_ref, pieces, gmat, w_ref, acc, top):
    z, y, x, c = place()
    ones = jnp.ones((16, HALF), BF)
    count = jnp.zeros((1, 128), F32)
    for b in range(16):
        for n in range(8):
            a = kv_ref[1, b, HALF + n * 8:HALF + (n + 1) * 8, :].astype(F32)
            count = count + a[3:4]
            hf, at = n // 4, (n % 4) * 128
            pieces[b * 8 + hf * 4:b * 8 + hf * 4 + 4, at:at + 128] = a[:4]
    docs0 = jnp.sum(count).astype(jnp.int32)
    gmat[...] = pieces[...].T.astype(BF)
    unit_of_row = lax.broadcasted_iota(jnp.int32, (128, HALF), 0) // 4
    piece_of_row = lax.broadcasted_iota(jnp.int32, (128, HALF), 0) % 4

    for i in range(4):
        hq = 2 * (4 * i + y) + lax.rem(c + i, 2)
        q = q_ref[i]
        none = jnp.zeros_like(q)
        q_pos = hq * HALF + lax.broadcasted_iota(jnp.int32, (1, HALF), 1)
        doc1 = jnp.where(q_pos >= docs0, -BIG, 0.0)
        w_ref[...] = jnp.where(piece_of_row == 3, doc1, -1.0)
        acc[...] = jnp.zeros_like(acc)
        top[...] = jnp.full_like(top, far_below)

        def unit(u, masked):
            b, hf = lax.div(u, 2), lax.rem(u, 2)
            lhs = jnp.concatenate([kv_ref[0, b, :HALF, :], gmat[...]], axis=1)
            sel = jnp.where(unit_of_row == u, w_ref[...], 0.0).astype(BF)
            first = hf == 0
            rhs = jnp.concatenate([jnp.where(first, q, none), jnp.where(first, none, q), sel], axis=0)
            s = jnp.dot(lhs, rhs, preferred_element_type=F32)
            if masked:
                key = lax.broadcasted_iota(jnp.int32, (HALF, HALF), 0)
                s = jnp.where(key <= lax.broadcasted_iota(jnp.int32, (HALF, HALF), 1), s, far_below)
            m_old = top[...]
            m_new = jnp.maximum(m_old, jnp.max(s, axis=0, keepdims=True))
            p = jnp.exp(s - m_new).astype(BF)
            shrink = jnp.exp(m_old - m_new)
            top[...] = m_new
            vt = jnp.concatenate(
                [kv_ref[1, b, pl.ds(pl.multiple_of(hf * 256 + n * 64, 64), 64), :] for n in range(4)], axis=1
            )
            vt = jnp.concatenate([vt, ones], axis=0)
            acc[...] = acc[...] * shrink + jnp.dot(vt, p, preferred_element_type=F32)

        start = jnp.where(hq * HALF >= docs0, lax.div(docs0, HALF), 0)

        def step(u, carry):
            unit(u, False)
            return carry

        lax.fori_loop(start, hq, step, 0)
        unit(hq, True)
        total = acc[...]
        o_ref[i] = (total[:HD] / total[HD:HD + 1]).astype(BF)


def attend(q, kv):
    return pl.pallas_call(
        attend_kernel,
        out_shape=sds((4, HD, HALF), BF),
        in_specs=[VM, VM],
        out_specs=VM,
        scratch_shapes=[
            pltpu.VMEM((128, HALF), F32),
            pltpu.VMEM((HALF, 128), BF),
            pltpu.VMEM((128, HALF), F32),
            pltpu.VMEM((80, HALF), F32),
            pltpu.VMEM((1, HALF), F32),
        ],
        compiler_params=pltpu.CompilerParams(vmem_limit_bytes=40 * 1024 * 1024),
        cost_estimate=pl.CostEstimate(flops=20_000_000_000, bytes_accessed=8_000_000, transcendentals=0),
        name="attend",
    )(q, kv)


def mix_kernel(
    att, wo_any, res, mid, a_in, wo, own, w_sem, a_s, a_r, o_l, m_sib, mr_sib, m_s_r, m_s_l, m_r
):
    z, y, x, c = place()
    sp, tp = z * 4 + y, x * 2 + c
    sib = dev(z, y, x, 1 - c)
    xp, xm, x2 = up(x, 1), up(x, 3), up(x, 2)
    head = 4 * x + z
    w_copy = pltpu.make_async_copy(wo_any, wo, w_sem.at[0])
    w_copy.start()
    pending = []
    for i in range(4):
        hf = lax.rem(c + i, 2)
        for k in range(4):
            to = 4 * hf + k
            mine = (z == i) & (to == tp)
            src = att.at[i, :, pl.ds(k * 128, 128)]
            dst = a_in.at[pl.ds(pl.multiple_of(head * HD, HD), HD)]
            local = pltpu.make_async_copy(src, dst, a_r.at[head])
            remote = send(src, dst, a_s.at[4 * i + k], a_r.at[head], (i * 4 + y, to))

            @pl.when(mine)
            def _():
                local.start()

            @pl.when(jnp.logical_not(mine))
            def _():
                remote.start()

            pending.append((mine, remote))
    for h in range(16):
        rows = pl.ds(h * HD, HD)
        send(a_in.at[rows], a_in.at[rows], a_s.at[0], a_r.at[h], sib).wait_recv()
    w_copy.wait()
    a = a_in[...].astype(F32).T.astype(BF)
    for n in range(4):
        cols = slice(n * 512, (n + 1) * 512)
        mixed = jnp.dot(a, wo[:, cols], preferred_element_type=F32)
        own[:, cols] = (res[:, cols].astype(F32) + mixed).astype(BF)

    done = []

    def go(copy):
        copy.start()
        done.append(copy)

    def rows_of(xs, cc, half):
        return pl.ds((2 * xs + cc) * 128 + half * 64, 64)

    locals_ = []
    for half in range(2):
        src, dst = own.at[pl.ds(half * 64, 64)], mid.at[rows_of(x, c, half)]
        n = 2 * x + half
        go(send(src, dst, m_s_r.at[n], m_r.at[n], dev(z, y, xp, c)))
        go(send(src, dst, m_s_l.at[n], m_r.at[n], dev(z, y, xm, c)))
        go(send(src, dst, m_sib.at[n], mr_sib.at[n], sib))
        loc = pltpu.make_async_copy(src, dst, o_l.at[half])
        loc.start()
        locals_.append(loc)

    def arrived(xs, half):
        rows, n = rows_of(xs, c, half), 2 * xs + half
        send(mid.at[rows], mid.at[rows], m_sib.at[n], m_r.at[n], sib).wait_recv()
        return rows, n

    def to_sib(rows, n):
        go(send(mid.at[rows], mid.at[rows], m_sib.at[n], mr_sib.at[n], sib))

    rows, n = arrived(xm, 0)
    go(send(mid.at[rows], mid.at[rows], m_s_r.at[n], m_r.at[n], dev(z, y, xp, c)))
    to_sib(rows, n)
    to_sib(*arrived(xp, 0))
    rows, n = arrived(xp, 1)
    go(send(mid.at[rows], mid.at[rows], m_s_l.at[n], m_r.at[n], dev(z, y, xm, c)))
    to_sib(rows, n)
    to_sib(*arrived(xm, 1))
    to_sib(*arrived(x2, 0))
    to_sib(*arrived(x2, 1))
    for n in range(8):
        rows = rows_of(n // 2, 1 - c, n % 2)
        send(mid.at[rows], mid.at[rows], m_sib.at[n], mr_sib.at[n], sib).wait_recv()
    for loc in locals_:
        loc.wait()
    for mine, remote in pending:
        @pl.when(jnp.logical_not(mine))
        def _():
            remote.wait_send()
    for copy in done:
        copy.wait_send()


def mix(att, wo, res):
    return pl.pallas_call(
        mix_kernel,
        out_shape=sds((T, D), BF),
        in_specs=[VM, HB, VM],
        out_specs=HB,
        scratch_shapes=[
            pltpu.VMEM((1024, 128), BF),
            pltpu.VMEM((1024, D), BF),
            pltpu.VMEM((128, D), BF),
            DMA((1,)), DMA((16,)), DMA((16,)), DMA((2,)),
            DMA((8,)), DMA((8,)), DMA((8,)), DMA((8,)), DMA((8,)),
        ],
        compiler_params=pltpu.CompilerParams(has_side_effects=True),
        cost_estimate=pl.CostEstimate(flops=20_000_000_000, bytes_accessed=8_000_000, transcendentals=0),
        name="mix",
    )(att, wo, res)


def scatter_kernel(
    part, mid, out, sibbuf, stage, hop_a, hop_b, from_l, from_r, res,
    mid_sem, s_sib, r_sib, s_hop, r_hop, s_out, r_l, r_r,
):
    z, y, x, c = place()
    tp = x * 2 + c
    sib = dev(z, y, x, 1 - c)
    right, left = dev(z, y, up(x, 1), c), dev(z, y, up(x, 3), c)
    m_copy = pltpu.make_async_copy(mid.at[:, pl.ds(pl.multiple_of(tp * 256, 256), 256)], res, mid_sem.at[0])
    m_copy.start()
    done = []

    def go(copy):
        copy.start()
        done.append(copy)

    for rel in (2, 1, 3, 0):
        xt = up(x, rel)
        cols = pl.ds(pl.multiple_of((2 * xt + 1 - c) * 256, 256), 256)
        go(send(part.at[:, cols], sibbuf.at[rel], s_sib.at[rel], r_sib.at[rel], sib))

    def chunks(lo, n, f):
        def one(k, carry):
            f(pl.ds(pl.multiple_of(lo + k * 128, 128), 128), pl.ds(pl.multiple_of(k * 128, 128), 128))
            return carry

        lax.fori_loop(0, n, one, 0)

    def pair(rel):
        send(sibbuf.at[rel], sibbuf.at[rel], s_sib.at[rel], r_sib.at[rel], sib).wait_recv()
        xt = up(x, rel)
        cols = pl.ds(pl.multiple_of((2 * xt + c) * 256, 256), 256)
        return lambda rows: part[rows, cols].astype(F32) + sibbuf[rel, rows, :].astype(F32)

    A, B = pl.ds(0, HALF), pl.ds(HALF, HALF)

    def put(rel, value):
        def f(rows, _):
            stage[rel, rows, :] = value(rows).astype(BF)

        return f

    two = pair(2)
    chunks(0, 8, put(2, two))
    go(send(stage.at[2, A], hop_a, s_hop.at[0], r_hop.at[0], right))
    go(send(stage.at[2, B], hop_b, s_hop.at[1], r_hop.at[1], left))
    one = pair(1)
    chunks(HALF, 4, put(1, one))
    go(send(stage.at[1, B], from_l.at[B], s_out.at[0], r_l.at[1], right))
    three = pair(3)
    chunks(0, 4, put(3, three))
    go(send(stage.at[3, A], from_r.at[A], s_out.at[1], r_r.at[0], left))

    send(hop_a, hop_a, s_hop.at[0], r_hop.at[0], sib).wait_recv()

    def fold_a(rows, rel):
        stage[1, rows, :] = (one(rows) + hop_a[rel, :].astype(F32)).astype(BF)

    chunks(0, 4, fold_a)
    go(send(stage.at[1, A], from_l.at[A], s_out.at[2], r_l.at[0], right))
    send(hop_b, hop_b, s_hop.at[1], r_hop.at[1], sib).wait_recv()

    def fold_b(rows, rel):
        stage[3, rows, :] = (three(rows) + hop_b[rel, :].astype(F32)).astype(BF)

    chunks(HALF, 4, fold_b)
    go(send(stage.at[3, B], from_r.at[B], s_out.at[3], r_r.at[1], left))
    mine = pair(0)
    m_copy.wait()
    send(from_l.at[B], from_l.at[B], s_out.at[0], r_l.at[1], sib).wait_recv()
    send(from_r.at[A], from_r.at[A], s_out.at[0], r_r.at[0], sib).wait_recv()
    send(from_l.at[A], from_l.at[A], s_out.at[0], r_l.at[0], sib).wait_recv()
    send(from_r.at[B], from_r.at[B], s_out.at[0], r_r.at[1], sib).wait_recv()

    def final(rows, _):
        feed = mine(rows) + from_l[rows, :].astype(F32) + from_r[rows, :].astype(F32)
        out[rows, :] = (res[rows, :].astype(F32) + feed).astype(BF)

    chunks(0, 8, final)
    for copy in done:
        copy.wait_send()


def scatter(part, mid):
    return pl.pallas_call(
        scatter_kernel,
        out_shape=sds((T, 256), BF),
        in_specs=[VM, HB],
        out_specs=VM,
        scratch_shapes=[
            pltpu.VMEM((4, T, 256), BF),
            pltpu.VMEM((4, T, 256), BF),
            pltpu.VMEM((HALF, 256), BF),
            pltpu.VMEM((HALF, 256), BF),
            pltpu.VMEM((T, 256), BF),
            pltpu.VMEM((T, 256), BF),
            pltpu.VMEM((T, 256), BF),
            DMA((1,)), DMA((4,)), DMA((4,)), DMA((2,)), DMA((2,)), DMA((4,)), DMA((2,)), DMA((2,)),
        ],
        compiler_params=pltpu.CompilerParams(has_side_effects=True),
        cost_estimate=pl.CostEstimate(flops=20_000_000_000, bytes_accessed=8_000_000, transcendentals=0),
        name="scatter",
    )(part, mid)


def body(queries, keys, values, cum_gates, doc_ids, residual, w_out, norm_gain, w_up, w_down):
    both = jnp.concatenate([w_up, jnp.transpose(w_down)], axis=1)
    whole = lax.all_gather(both, "sp", axis=0, tiled=True)
    up_w, down_t = whole[:, :1024], whole[:, 1024:]
    qt, kv = pack(queries, keys, values, jnp.transpose(cum_gates), doc_ids.reshape(1, T))
    gain8 = jnp.broadcast_to(norm_gain.astype(F32)[None], (8, 256))
    qin, kvall, woall, resin, gainall = exchange(qt, kv, w_out, residual, gain8)
    att = attend(qin, kvall)
    mid = mix(att, woall, resin)
    wide = mid.astype(F32)
    scaled = wide * lax.rsqrt(jnp.mean(wide * wide, axis=-1, keepdims=True) + eps)
    normed = (scaled * gainall[0:1]).astype(BF)
    up_proj = jnp.dot(normed, up_w, preferred_element_type=F32)
    hidden = jnp.square(jax.nn.relu(up_proj)).astype(BF)
    part = lax.dot_general(hidden, down_t, (((1,), (1,)), ((), ())), preferred_element_type=F32).astype(BF)
    return scatter(part, mid)


def solution(mesh):
    in_specs = (
        P("sp", "tp"),
        P("sp", "tp"),
        P("sp", "tp"),
        P("sp", "tp"),
        P("sp"),
        P("sp", "tp"),
        P("tp", None),
        P("tp"),
        P("sp", "tp"),
        P("tp", "sp"),
    )
    return jax.shard_map(body, mesh=mesh, in_specs=in_specs, out_specs=P("sp", "tp"), check_vma=False)
```

time: 397 us -> 205 us (0.52); the launches traced: 401 us -> 204 us
  waiting for transfers between devices: 226 us -> 0.04 us
  Pallas kernels: 0 us -> 162 us
  blocking collectives: 55.6 us -> 0 us
  loops' own time: 31.5 us -> 0 us
  local copies, waits for them, and re-layouts: 27.4 us -> 9.08 us
  starting transfers between devices: 16.1 us -> 0.01 us
  matrix products: 21.1 us -> 14.6 us
  other arithmetic: 10.2 us -> 4.86 us
    all_gather x3 -> x1, waiting for transfers between devices: 181 us -> 0.02 us  [body(): whole = lax.all_gather(both, 'sp', axis=0, tiled=True)]
    pallas_call x0 -> x5, Pallas kernels: none -> 162 us  [the longest x1 57.6 us: mix(): pl.pallas_call(mix_kernel, out_shape=sds((T, D), BF), in_specs=[VM, HB, V...]
    reduce_scatter x1 -> x0, waiting for transfers between devices: 39 us -> none  [body(): lax.psum_scatter(down_terms.astype(jnp.bfloat16), 'tp', scatter_dimension...]
    another operation x17 -> x0, loops' own time: 31.5 us -> none  [the longest x1 31.2 us: fold_piece(): return lax.fori_loop(0, piece_rows // key_span, key_step, state_carry)]
    all_to_all x1 -> x0, blocking collectives: 31.3 us -> none  [copy_for_each(): lax.all_to_all(jnp.broadcast_to(value[None], (peers, *value.shape)), axis...]
    all_gather x1 -> x0, blocking collectives: 24.3 us -> none  [body(): lax.all_gather(doc_ids, 'sp', axis=0, tiled=True)]
    slice x19 -> x1, local copies, waits for them, and re-layouts: 16.8 us -> 0.85 us  [body(): normed = (scaled * gainall[0:1]).astype(BF)]
    all_to_all x3 -> x0, starting transfers between devices: 15.8 us -> none  [the longest x2 11.5 us: copy_for_each(): lax.all_to_all(jnp.broadcast_to(value[None], (peers, *value.shape)), axis...]
  transfers between devices with their start and end apart: 7 -> 1, of which waited for: 4 -> 0; matrix products, arithmetic and copies ran while one was open for 10% -> 3% of each run, Pallas kernels for 0% -> 63%
where the time goes in v1:
time: 205 us; the launch traced here: 204 us
  Pallas kernels  162 us (79%)
  matrix products  14.6 us (7%)
  between operations  13.5 us (7%)
  local copies, waits for them, and re-layouts  9.08 us (4%)
  other arithmetic  4.86 us (2%)
    pallas_call x1, Pallas kernels, mix(): pl.pallas_call(mix_kernel, out_shape=sds((T, D), BF), in_specs=[VM, HB, V...  57.6 us
    pallas_call x1, Pallas kernels, exchange(): pl.pallas_call(exchange_kernel, out_shape=(sds((4, HD, HALF), BF), sds((2...  48.4 us
    pallas_call x1, Pallas kernels, scatter(): pl.pallas_call(scatter_kernel, out_shape=sds((T, 256), BF), in_specs=[VM,...  33.9 us
    pallas_call x1, Pallas kernels, attend(): pl.pallas_call(attend_kernel, out_shape=sds((4, HD, HALF), BF), in_specs=...  20.1 us
    dot_general x1, matrix products, body(): lax.dot_general(hidden, down_t, (((1,), (1,)), ((), ())), preferred_eleme...  14.6 us
    unnamed x8, local copies, waits for them, and re-layouts  6.98 us
  transfers between devices with their start and end apart: 1, of which 0 were waited for; matrix products, arithmetic and copies ran while one was open for 3% of the time, Pallas kernels for 63%

profile of v1, /device:TPU:0, one launch (start us, length us, event | category | flops | bytes accessed | tf_op | source)
XLA Modules:
  0.0 204.4 jit_solution(1662542722332472317)
XLA Ops:
  6.5 0.0 all-gather.2.cloned.1.call-start
  6.5 1.1 copy.11
  7.7 1.8 pad_maximum_fusion
  9.4 0.0 all-gather.2.cloned.1.call-update
  9.5 2.3 %pack.1 = (bf16[2,64,1024]{2,1,0:T(8,128)(2,1)}, bf16[2,2,576,128]{3,2,1,0:T(8,128)(2,1)}) custom-call(bf16[1024,128]{1,0:T(8,128)(2,1)} %q_ref.1, bf16[1024,128]{1,0:T(8,128)(2,1)} %k_ref.1, bf16[1024,128]{1,0:T(8,128)(2,1)} %v_ref.1, f32[2,1024]{1,0:T(2,128)} %bitcast.5, s32[1,1024]{1,0:T(1,128)} %bitcast.7), custom_call_target="tpu_custom_call" | custom-call | tf_op jit(solution)/shard_map/pack/pallas_call | solution.py:75
  11.7 1.3 broadcast_in_dim.2.gain
  13.0 48.4 %exchange.1 = (bf16[4,64,512]{2,1,0:T(8,128)(2,1)}, bf16[2,16,576,128]{3,2,1,0:T(8,128)(2,1)}, bf16[1024,2048]{1,0:T(8,128)(2,1)}, bf16[128,2048]{1,0:T(8,128)(2,1)}, f32[8,2048]{1,0:T(8,128)}) custom-call(bf16[2,64,1024]{2,1,0:T(8,128)(2,1)} %get-tuple-element.12.qt, bf16[2,2,576,128]{3,2,1,0:T(8,128)(2,1)} %get-tuple-element.13.kv, bf16[128,2048]{1,0:T(8,128)(2,1)} %wo.1, ...), custom_call_target="tpu_custom_call" | custom-call | flops 20000000000 | bytes 16000000 | tf_op jit(solution)/shard_map/exchange/pallas_call | solution.py:234
  61.4 0.8 slice.9
  62.3 0.0 copy-start
  62.3 2.3 %copy-done = bf16[2,16,576,128]{3,2,1,0:T(8,128)(2,1)S(1)} copy-done((bf16[2,16,576,128]{3,2,1,0:T(8,128)(2,1)S(1)}, bf16[2,16,576,128]{3,2,1,0:T(8,128)(2,1)}, u32[]{:S(2)}) %copy-start) | copy-done | bytes 4718616
  64.6 0.0 copy-start.2
  64.6 0.9 copy-done.2
  65.6 20.1 %attend.1.att = bf16[4,64,512]{2,1,0:T(8,128)(2,1)S(1)} custom-call(bf16[4,64,512]{2,1,0:T(8,128)(2,1)S(1)} %copy-done.2, bf16[2,16,576,128]{3,2,1,0:T(8,128)(2,1)S(1)} %copy-done), custom_call_target="tpu_custom_call" | custom-call | flops 20000000000 | bytes 8000000 | tf_op jit(solution)/shard_map/attend/pallas_call | solution.py:315
  85.7 0.0 copy-start.1
  85.7 0.7 copy-done.1
  86.4 57.6 %mix.1.mid = bf16[1024,2048]{1,0:T(8,128)(2,1)} custom-call(bf16[4,64,512]{2,1,0:T(8,128)(2,1)} %copy-done.1, bf16[1024,2048]{1,0:T(8,128)(2,1)} %get-tuple-element.16.wo_any, bf16[128,2048]{1,0:T(8,128)(2,1)} %get-tuple-element.17.res), custom_call_target="tpu_custom_call" | custom-call | flops 20000000000 | bytes 8000000 | tf_op jit(solution)/shard_map/mix/pallas_call | solution.py:425
  144.0 3.1 %fusion = f32[1024]{0:T(1024)S(1)} fusion(bf16[1024,2048]{1,0:T(8,128)(2,1)} %mix.1.mid), kind=kLoop, calls=%fused_computation.2 | loop fusion | flops 6290432 | bytes 4198400 | tf_op jit(solution)/shard_map/reduce_sum | solution.py:558
  147.1 0.0 all-gather.2.cloned.1.call-done
  147.2 14.6 %fusion.10.part = bf16[1024,2048]{1,0:T(8,128)(2,1)} fusion(bf16[2048,2048]{0,1:T(8,128)(2,1)} %all-gather.2.cloned.1.call-done, bf16[1024,2048]{1,0:T(8,128)(2,1)} %mix.1.mid, f32[2048]{0:T(1024)S(1)} %bitcast.6, f32[1024]{0:T(1024)S(1)} %add_rsqrt_fusion), kind=kOutput, calls=%fused_computation.12 | convolution fusion | flops 8603566080 | bytes 16789504 | tf_op jit(solution)/shard_map/dot_general | solution.py:562
  161.8 33.9 %scatter.1 = bf16[1024,256]{1,0:T(8,128)(2,1)} custom-call(bf16[1024,2048]{1,0:T(8,128)(2,1)} %fusion.10.part, bf16[1024,2048]{1,0:T(8,128)(2,1)} %mix.1.mid), custom_call_target="tpu_custom_call" | custom-call | flops 20000000000 | bytes 8000000 | tf_op jit(solution)/shard_map/scatter/pallas_call | solution.py:527
  195.6 1.9 copy.13
  (1 shorter events, 0.0 us)
Async XLA Ops:
  6.5 140.6 %all-gather.2.cloned.1.call-start = ((), (), s32[]{:S(2)}) async-start(), calls=%async_computation | async-start | bytes 8912896 | tf_op jit(solution)/shard_map/all_gather | solution.py:550
  62.3 2.3 %copy-start = (bf16[2,16,576,128]{3,2,1,0:T(8,128)(2,1)S(1)}, bf16[2,16,576,128]{3,2,1,0:T(8,128)(2,1)}, u32[]{:S(2)}) copy-start(bf16[2,16,576,128]{3,2,1,0:T(8,128)(2,1)} %get-tuple-element.15.kv_ref) | copy-start | bytes 14155780
  64.6 0.9 copy-start.2
  85.7 0.7 copy-start.1
Sparse Core Ops, SparseCore 0:
  9.6 84.6 all-gather.1
